TPU v7x, 128 devices: a whole 4x4x4 slice. The times are simulated.
128 devices in a mesh: sp: 32 (over y, x, core), tp: 4 (over z).
Axes of the slice: x: 4, y: 4, z: 4, core: 2. Of those that a mesh axis runs over, the one named last changes fastest.
Arguments:
- sequence: bfloat16 [4, 1024, 1024], P(None, 'sp', 'tp'), may hold values from -6 to 6
- norm_gain: float32 [3, 1024], replicated, may hold values from 0.1 to 1.9
- weight_value: bfloat16 [3, 1024, 512], P(None, 'sp', 'tp'), may hold values from -0.1875 to 0.1875
- weight_outer: bfloat16 [3, 1024, 512], P(None, 'sp', 'tp'), may hold values from -0.1875 to 0.1875
- weight_inner: bfloat16 [3, 1024, 512], P(None, 'sp', 'tp'), may hold values from -0.1875 to 0.1875
- conv_taps: float32 [3, 3, 512], P(None, None, 'tp'), may hold values from -3 to 3
- weight_out: bfloat16 [3, 512, 1024], P(None, 'tp', 'sp'), may hold values from -0.25 to 0.25
Outputs:
- mixed: bfloat16 [4, 1024, 1024], P(None, 'sp', 'tp')
All inputs are finite; a program needn't handle non-finite values.
Results may differ from a plain program's by a relative error of at most 0.03.
Values may be sent and summed in bfloat16 or wider, within the bound.
A program may use at most 64 MiB of HBM per device.

v0:
```python
import jax
import jax.numpy as jnp
from jax import lax
from jax.sharding import PartitionSpec as P

LAYERS = 3


def folded(array, axis, dim, update, carry):
    whole = jax.tree.map(lambda part: lax.all_gather(part, axis, axis=dim, tiled=True), array)
    return update(carry, whole, jnp.int32(0))


def from_behind(value, axis, steps):
    count = lax.axis_size(axis)
    first, last = (max(0, -steps), min(count, count - steps))
    return lax.ppermute(value, axis, [(source, source + steps) for source in range(first, last)])


def over_all(slab, axis, dim, apply):
    everything = lax.all_gather(slab, axis, axis=dim, tiled=True)
    return apply(everything, jnp.int32(0))


def rms_rows(values, gain_row):
    wide = values.astype(jnp.float32)
    scaled = wide * lax.rsqrt(jnp.mean(wide * wide, axis=-1, keepdims=True) + 1e-06)
    return (scaled * gain_row).astype(jnp.bfloat16)


def body(sequence, norm_gain, weight_value, weight_outer, weight_inner, conv_taps, weight_out):
    current = sequence
    seq_count = sequence.shape[0]
    local_len = sequence.shape[1]
    channels = weight_value.shape[2]
    depth = conv_taps.shape[1]
    for layer_index in range(LAYERS):
        whole = lax.all_gather(current, "tp", axis=2, tiled=True)
        normed = rms_rows(whole, norm_gain[layer_index]).reshape(
            seq_count * local_len, whole.shape[2]
        )
        empty = jnp.zeros((normed.shape[0], channels), jnp.float32)

        def add_rows(running, weight_rows, offset):
            columns = lax.dynamic_slice_in_dim(normed, offset, weight_rows.shape[0], 1)
            return running + jnp.dot(columns, weight_rows, preferred_element_type=jnp.float32)

        sum_value = folded(weight_value[layer_index], "sp", 0, add_rows, empty)
        sum_outer = folded(weight_outer[layer_index], "sp", 0, add_rows, empty)
        sum_inner = folded(weight_inner[layer_index], "sp", 0, add_rows, empty)
        proj_value = sum_value.astype(jnp.bfloat16)
        proj_outer = sum_outer.astype(jnp.bfloat16)
        proj_inner = sum_inner.astype(jnp.bfloat16)
        product = (proj_inner.astype(jnp.float32) * proj_value.astype(jnp.float32)).reshape(
            seq_count, local_len, channels
        )
        last_rows = product[:, local_len - (depth - 1) :, :]
        before = from_behind(last_rows, "sp", 1)
        padded = jnp.concatenate([before, product], axis=1)
        filtered = conv_taps[layer_index, 0] * padded[:, 0:local_len]
        for offset in range(1, depth):
            filtered = (
                filtered + conv_taps[layer_index, offset] * padded[:, offset : offset + local_len]
            )
        gated = (
            proj_outer.astype(jnp.float32).reshape(seq_count, local_len, channels) * filtered
        ).astype(jnp.bfloat16)
        gated_rows = gated.reshape(seq_count * local_len, channels)

        def project_columns(weight_cols, offset):
            return jnp.dot(gated_rows, weight_cols, preferred_element_type=jnp.float32)

        terms = over_all(weight_out[layer_index], "sp", 1, project_columns)
        shares = lax.psum_scatter(
            terms.astype(jnp.bfloat16), "tp", scatter_dimension=1, tiled=True
        ).astype(jnp.float32)
        shares = shares.reshape(seq_count, local_len, shares.shape[1])
        current = (current.astype(jnp.float32) + shares).astype(jnp.bfloat16)
    return current


def solution(mesh):
    return jax.shard_map(
        body,
        mesh=mesh,
        in_specs=(
            P(None, "sp", "tp"),
            P(),
            P(None, "sp", "tp"),
            P(None, "sp", "tp"),
            P(None, "sp", "tp"),
            P(None, None, "tp"),
            P(None, "tp", "sp"),
        ),
        out_specs=P(None, "sp", "tp"),
        check_vma=False,
    )
```

profile of v0, /device:TPU:0, one launch (start us, length us, event | category | flops | bytes accessed | tf_op | source)
XLA Modules:
  0.0 380.7 jit_solution(10216382479463195660)
XLA Ops:
  6.5 0.8 fusion.58
  7.4 13.8 %all_gather.45 = bf16[4,32,1024]{2,1,0:T(8,128)(2,1)S(1)} all-gather(bf16[4,32,256]{2,1,0:T(8,128)(2,1)} %param.7), channel_id=1, replica_groups=mesh['sp'=32,'tp'=4] {'tp'}, dimensions={2}, use_global_device_ids=true | all-gather | bytes 327680 | tf_op jit(solution)/shard_map/all_gather | solution.py:38
  21.3 0.6 copy-done.1
  21.9 25.3 %all-gather.1 = bf16[1,1024,128]{2,1,0:T(8,128)(2,1)S(1)} all-gather(bf16[1,32,128]{2,1,0:T(8,128)(2,1)S(1)} %get-tuple-element.15), channel_id=3, replica_groups=mesh['sp'=32,'tp'=4] {'sp'}, dimensions={1}, use_global_device_ids=true | all-gather | bytes 270336 | tf_op jit(solution)/shard_map/all_gather | solution.py:10
  47.2 24.2 %all-gather.2 = bf16[1,1024,128]{2,1,0:T(8,128)(2,1)S(1)} all-gather(bf16[1,32,128]{2,1,0:T(8,128)(2,1)S(1)} %get-tuple-element.12), channel_id=4, replica_groups=mesh['sp'=32,'tp'=4] {'sp'}, dimensions={1}, use_global_device_ids=true | all-gather | bytes 270336 | tf_op jit(solution)/shard_map/all_gather | solution.py:10
  72.0 2.3 collective-permute-start
  74.3 22.6 %all-gather = bf16[1,1024,128]{2,1,0:T(8,128)(2,1)S(1)} all-gather(bf16[1,32,128]{2,1,0:T(8,128)(2,1)S(1)} %get-tuple-element.9), channel_id=2, replica_groups=mesh['sp'=32,'tp'=4] {'sp'}, dimensions={1}, use_global_device_ids=true | all-gather | bytes 270336 | tf_op jit(solution)/shard_map/all_gather | solution.py:10
  97.1 0.5 copy-done.5
  97.7 24.2 %all-gather.3 = bf16[1,128,1024]{1,2,0:T(8,128)(2,1)S(1)} all-gather(bf16[1,128,32]{1,2,0:T(8,128)(2,1)S(1)} %get-tuple-element.6), channel_id=5, replica_groups=mesh['sp'=32,'tp'=4] {'sp'}, dimensions={2}, use_global_device_ids=true | all-gather | bytes 270336 | tf_op jit(solution)/shard_map/all_gather | solution.py:21
  121.9 0.9 convolution_convert_fusion.2
  122.9 22.6 %all-gather.5 = bf16[1,1024,128]{2,1,0:T(8,128)(2,1)S(1)} all-gather(bf16[1,32,128]{2,1,0:T(8,128)(2,1)S(1)} %get-tuple-element.16), channel_id=7, replica_groups=mesh['sp'=32,'tp'=4] {'sp'}, dimensions={1}, use_global_device_ids=true | all-gather | bytes 270336 | tf_op jit(solution)/shard_map/all_gather | solution.py:10
  145.6 24.2 %all-gather.6 = bf16[1,1024,128]{2,1,0:T(8,128)(2,1)S(1)} all-gather(bf16[1,32,128]{2,1,0:T(8,128)(2,1)S(1)} %get-tuple-element.13), channel_id=8, replica_groups=mesh['sp'=32,'tp'=4] {'sp'}, dimensions={1}, use_global_device_ids=true | all-gather | bytes 270336 | tf_op jit(solution)/shard_map/all_gather | solution.py:10
  169.8 22.8 %all-gather.4 = bf16[1,1024,128]{2,1,0:T(8,128)(2,1)S(1)} all-gather(bf16[1,32,128]{2,1,0:T(8,128)(2,1)S(1)} %get-tuple-element.10), channel_id=6, replica_groups=mesh['sp'=32,'tp'=4] {'sp'}, dimensions={1}, use_global_device_ids=true | all-gather | bytes 270336 | tf_op jit(solution)/shard_map/all_gather | solution.py:10
  192.5 24.3 %all-gather.7 = bf16[1,128,1024]{1,2,0:T(8,128)(2,1)S(1)} all-gather(bf16[1,128,32]{1,2,0:T(8,128)(2,1)S(1)} %get-tuple-element.7), channel_id=9, replica_groups=mesh['sp'=32,'tp'=4] {'sp'}, dimensions={2}, use_global_device_ids=true | all-gather | bytes 270336 | tf_op jit(solution)/shard_map/all_gather | solution.py:21
  216.9 0.9 fusion.32
  217.7 12.3 %all_gather.50 = bf16[4,32,1024]{2,1,0:T(8,128)(2,1)S(1)} all-gather(bf16[4,32,256]{2,1,0:T(8,128)(2,1)S(1)} %fusion.32), channel_id=1, replica_groups=mesh['sp'=32,'tp'=4] {'tp'}, dimensions={2}, use_global_device_ids=true | all-gather | bytes 327680 | tf_op jit(solution)/shard_map/all_gather | solution.py:38
  230.8 1.3 collective-permute-start.1
  232.0 0.2 convolution_convert_fusion.8
  232.3 0.6 collective-permute-done.1
  232.9 0.9 convolution_convert_fusion.1
  233.9 27.6 %all-gather.9 = bf16[1,1024,128]{2,1,0:T(8,128)(2,1)S(1)} all-gather(bf16[1,32,128]{2,1,0:T(8,128)(2,1)S(1)} %get-tuple-element.14), channel_id=11, replica_groups=mesh['sp'=32,'tp'=4] {'sp'}, dimensions={1}, use_global_device_ids=true | all-gather | bytes 270336 | tf_op jit(solution)/shard_map/all_gather | solution.py:10
  261.5 23.0 %all-gather.10 = bf16[1,1024,128]{2,1,0:T(8,128)(2,1)S(1)} all-gather(bf16[1,32,128]{2,1,0:T(8,128)(2,1)S(1)} %get-tuple-element.11), channel_id=12, replica_groups=mesh['sp'=32,'tp'=4] {'sp'}, dimensions={1}, use_global_device_ids=true | all-gather | bytes 270336 | tf_op jit(solution)/shard_map/all_gather | solution.py:10
  284.4 23.8 %all-gather.8 = bf16[1,1024,128]{2,1,0:T(8,128)(2,1)S(1)} all-gather(bf16[1,32,128]{2,1,0:T(8,128)(2,1)S(1)} %get-tuple-element.8), channel_id=10, replica_groups=mesh['sp'=32,'tp'=4] {'sp'}, dimensions={1}, use_global_device_ids=true | all-gather | bytes 270336 | tf_op jit(solution)/shard_map/all_gather | solution.py:10
  308.3 23.0 %all-gather.11 = bf16[1,128,1024]{1,2,0:T(8,128)(2,1)S(1)} all-gather(bf16[1,128,32]{1,2,0:T(8,128)(2,1)S(1)} %get-tuple-element.5), channel_id=13, replica_groups=mesh['sp'=32,'tp'=4] {'sp'}, dimensions={2}, use_global_device_ids=true | all-gather | bytes 270336 | tf_op jit(solution)/shard_map/all_gather | solution.py:21
  331.2 0.9 fusion.31
  332.1 12.3 %all_gather.55 = bf16[4,32,1024]{2,1,0:T(8,128)(2,1)S(1)} all-gather(bf16[4,32,256]{2,1,0:T(8,128)(2,1)S(1)} %fusion.31), channel_id=1, replica_groups=mesh['sp'=32,'tp'=4] {'tp'}, dimensions={2}, use_global_device_ids=true | all-gather | bytes 327680 | tf_op jit(solution)/shard_map/all_gather | solution.py:38
  345.1 1.3 collective-permute-start.2
  346.4 0.2 convolution_convert_fusion.5
  346.6 0.6 collective-permute-done.2
  347.3 0.9 convolution_convert_fusion
  348.2 24.5 %reduce-scatter.8.cloned.1.call-done = bf16[128,256]{1,0:T(8,128)(2,1)} async-done(((bf16[128,1024]{1,0:T(8,128)(2,1)}), bf16[128,256]{1,0:T(8,128)(2,1)}) %reduce-scatter.8.cloned.1.call-update) | async-done | bytes 65552 | tf_op jit(solution)/shard_map/reduce_scatter | solution.py:74
  372.7 1.5 fusion.30
  (46 shorter events, 2.7 us)
Async XLA Ops:
  6.5 210.3 %reduce-scatter.4.cloned.1.call-start = ((), (), s32[]{:S(2)}) async-start(), calls=%async_computation.3 | async-start | bytes 327680 | tf_op jit(solution)/shard_map/reduce_scatter | solution.py:74
  21.2 0.7 copy-start.1
  21.9 25.3 %copy-start.2 = (bf16[3,32,128]{2,1,0:T(8,128)(2,1)S(1)}, bf16[3,32,128]{2,1,0:T(8,128)(2,1)}, u32[]{:S(2)}) copy-start(bf16[3,32,128]{2,1,0:T(8,128)(2,1)} %param.9) | copy-start | bytes 73732
  71.7 2.5 copy-start.3
  72.0 49.9 %collective-permute-start = (f32[4,2,128]{2,1,0:T(2,128)S(1)}, f32[4,2,128]{2,1,0:T(2,128)S(1)}, u32[]{:S(2)}, u32[]{:S(2)}) collective-permute-start(f32[4,2,128]{2,1,0:T(2,128)S(1)} %slice.132), channel_id=1, source_target_pairs={{0,4},{4,8},{8,12},{12,16},{16,20},{20,24},{24,28},{28,32},{32,36}... | collective-permute-start | bytes 12296 | tf_op jit(solution)/shard_map/ppermute | solution.py:17
  96.9 0.7 copy-start.5
  96.9 0.8 copy-start.4
  122.9 208.4 %reduce-scatter.6.cloned.1.call-start = ((), (), s32[]{:S(2)}) async-start(), calls=%async_computation.4 | async-start | bytes 327680 | tf_op jit(solution)/shard_map/reduce_scatter | solution.py:74
  192.5 24.3 %copy-start = (bf16[4,32,256]{2,1,0:T(8,128)(2,1)S(1)}, bf16[4,32,256]{2,1,0:T(8,128)(2,1)}, u32[]{:S(2)}) copy-start(bf16[4,32,256]{2,1,0:T(8,128)(2,1)} %param.7) | copy-start | bytes 196612
  230.8 2.1 collective-permute-start.1
  233.8 138.8 %reduce-scatter.8.cloned.1.call-start = ((), (), s32[]{:S(2)}) async-start(), calls=%async_computation.5 | async-start | bytes 327680 | tf_op jit(solution)/shard_map/reduce_scatter | solution.py:74
  345.1 2.1 collective-permute-start.2
Sparse Core Ops, SparseCore 0:
  123.0 19.6 reduce-scatter.3
  234.0 23.3 reduce-scatter.5
  348.3 24.3 reduce-scatter.7
where the time goes:
time: 382 us; the launch traced here: 381 us
  blocking collectives  326 us (85%)
  waiting for transfers between devices  25.7 us (7%)
  between operations  13.3 us (3%)
  starting transfers between devices  4.92 us (1%)
  matrix products  4.77 us (1%)
  other arithmetic  4.11 us (1%)
    all_gather x9, blocking collectives, folded(): lax.all_gather(part, axis, axis=dim, tiled=True)  216 us
    all_gather x3, blocking collectives, over_all(): everything = lax.all_gather(slab, axis, axis=dim, tiled=True)  71.5 us
    all_gather x3, blocking collectives, body(): whole = lax.all_gather(current, 'tp', axis=2, tiled=True)  38.3 us
    reduce_scatter x3, waiting for transfers between devices, body(): lax.psum_scatter(terms.astype(jnp.bfloat16), 'tp', scatter_dimension=1, t...  24.5 us
  transfers between devices with their start and end apart: 6, of which 3 were waited for; matrix products, arithmetic and copies ran while one was open for 0% of the time, Pallas kernels for 0%

commit v1 on v0

--- a/solution.py
+++ b/solution.py
@@ -2,6 +2,7 @@
 import jax.numpy as jnp
 from jax import lax
 from jax.sharding import PartitionSpec as P
+from jax.lax import all_to_all, psum
 
 LAYERS = 3
 
@@ -35,7 +36,8 @@
     channels = weight_value.shape[2]
     depth = conv_taps.shape[1]
     for layer_index in range(LAYERS):
-        whole = lax.all_gather(current, "tp", axis=2, tiled=True)
+        block_out = jnp.concatenate(psum(1, "tp") * [current], axis=2)
+        whole = all_to_all(block_out, "tp", 2, 2, tiled=True)
         normed = rms_rows(whole, norm_gain[layer_index]).reshape(
             seq_count * local_len, whole.shape[2]
         )

time: 382 us -> 414 us (1.084)
  waiting for transfers between devices: 25.7 us -> 70.3 us
  blocking collectives: 326 us -> 288 us
  starting transfers between devices: 4.92 us -> 19.2 us
  local copies, waits for them, and re-layouts: 2.01 us -> 11.1 us
    reduce_scatter x3, waiting for transfers between devices: 24.5 us -> 68.5 us  [body(): lax.psum_scatter(terms.astype(jnp.bfloat16), 'tp', scatter_dimension=1, t...]
    all_gather x3 -> x0, blocking collectives: 38.3 us -> none  [body(): whole = lax.all_gather(current, 'tp', axis=2, tiled=True)]
    all_to_all x0 -> x3, starting transfers between devices: none -> 12.4 us  [body(): whole = all_to_all(block_out, 'tp', 2, 2, tiled=True)]
    unnamed x12 -> x20, local copies, waits for them, and re-layouts: 1.13 us -> 7.2 us
  transfers between devices with their start and end apart: 6 -> 9, of which waited for: 3 -> 6; matrix products, arithmetic and copies ran while one was open for 0% -> 0% of each run, Pallas kernels for 0% -> 0%
where the time goes in v1:
time: 414 us; the launch traced here: 412 us
  blocking collectives  288 us (70%)
  waiting for transfers between devices  70.3 us (17%)
  starting transfers between devices  19.2 us (5%)
  between operations  13.4 us (3%)
  local copies, waits for them, and re-layouts  11.1 us (3%)
  other arithmetic  5.17 us (1%)
  matrix products  4.76 us (1%)
    all_gather x9, blocking collectives, folded(): lax.all_gather(part, axis, axis=dim, tiled=True)  216 us
    all_gather x3, blocking collectives, over_all(): everything = lax.all_gather(slab, axis, axis=dim, tiled=True)  72.6 us
    reduce_scatter x3, waiting for transfers between devices, body(): lax.psum_scatter(terms.astype(jnp.bfloat16), 'tp', scatter_dimension=1, t...  68.5 us
    all_to_all x3, starting transfers between devices, body(): whole = all_to_all(block_out, 'tp', 2, 2, tiled=True)  12.4 us
  transfers between devices with their start and end apart: 9, of which 6 were waited for; matrix products, arithmetic and copies ran while one was open for 0% of the time, Pallas kernels for 0%

profile of v1, /device:TPU:0, one launch (start us, length us, event | category | flops | bytes accessed | tf_op | source)
XLA Modules:
  0.0 412.4 jit_solution(10823604273945362923)
XLA Ops:
  6.5 1.0 pad_maximum_fusion
  8.3 1.7 reshape.135
  9.9 5.5 %all-to-all-start = ((bf16[4,2,16384]{2,1,0:T(2,128)(2,1)}), bf16[4,2,16384]{2,1,0:T(2,128)(2,1)S(1)}, u32[]{:S(2)}, u32[]{:S(2)}) async-start(bf16[4,2,16384]{2,1,0:T(2,128)(2,1)} %reshape.135), calls=%async_computation | async-start | bytes 524288 | tf_op jit(solution)/shard_map/all_to_all | solution.py:40
  15.5 0.7 copy-done.1
  16.2 25.3 %all-gather.1 = bf16[1,1024,128]{2,1,0:T(8,128)(2,1)S(1)} all-gather(bf16[1,32,128]{2,1,0:T(8,128)(2,1)S(1)} %get-tuple-element.15), channel_id=3, replica_groups=mesh['sp'=32,'tp'=4] {'sp'}, dimensions={1}, use_global_device_ids=true | all-gather | bytes 270336 | tf_op jit(solution)/shard_map/all_gather | solution.py:11
  41.5 24.2 %all-gather.2 = bf16[1,1024,128]{2,1,0:T(8,128)(2,1)S(1)} all-gather(bf16[1,32,128]{2,1,0:T(8,128)(2,1)S(1)} %get-tuple-element.12), channel_id=4, replica_groups=mesh['sp'=32,'tp'=4] {'sp'}, dimensions={1}, use_global_device_ids=true | all-gather | bytes 270336 | tf_op jit(solution)/shard_map/all_gather | solution.py:11
  65.7 22.6 %all-gather = bf16[1,1024,128]{2,1,0:T(8,128)(2,1)S(1)} all-gather(bf16[1,32,128]{2,1,0:T(8,128)(2,1)S(1)} %get-tuple-element.9), channel_id=2, replica_groups=mesh['sp'=32,'tp'=4] {'sp'}, dimensions={1}, use_global_device_ids=true | all-gather | bytes 270336 | tf_op jit(solution)/shard_map/all_gather | solution.py:11
  88.4 24.2 %all-gather.3 = bf16[1,128,1024]{1,2,0:T(8,128)(2,1)S(1)} all-gather(bf16[1,128,32]{1,2,0:T(8,128)(2,1)S(1)} %get-tuple-element.6), channel_id=5, replica_groups=mesh['sp'=32,'tp'=4] {'sp'}, dimensions={2}, use_global_device_ids=true | all-gather | bytes 270336 | tf_op jit(solution)/shard_map/all_gather | solution.py:22
  114.5 2.3 collective-permute-start
  117.6 0.9 convolution_convert_fusion.2
  118.6 22.9 %reduce-scatter.4.cloned.1.call-done = bf16[128,256]{1,0:T(8,128)(2,1)} async-done(((bf16[128,1024]{1,0:T(8,128)(2,1)}), bf16[128,256]{1,0:T(8,128)(2,1)}) %reduce-scatter.4.cloned.1.call-update) | async-done | bytes 65552 | tf_op jit(solution)/shard_map/reduce_scatter | solution.py:76
  141.5 0.9 fusion.32
  143.1 1.7 reshape.137
  144.7 3.4 all-to-all-start.1
  148.2 25.0 %all-gather.5 = bf16[1,1024,128]{2,1,0:T(8,128)(2,1)S(1)} all-gather(bf16[1,32,128]{2,1,0:T(8,128)(2,1)S(1)} %get-tuple-element.16), channel_id=7, replica_groups=mesh['sp'=32,'tp'=4] {'sp'}, dimensions={1}, use_global_device_ids=true | all-gather | bytes 270336 | tf_op jit(solution)/shard_map/all_gather | solution.py:11
  173.2 24.2 %all-gather.6 = bf16[1,1024,128]{2,1,0:T(8,128)(2,1)S(1)} all-gather(bf16[1,32,128]{2,1,0:T(8,128)(2,1)S(1)} %get-tuple-element.13), channel_id=8, replica_groups=mesh['sp'=32,'tp'=4] {'sp'}, dimensions={1}, use_global_device_ids=true | all-gather | bytes 270336 | tf_op jit(solution)/shard_map/all_gather | solution.py:11
  197.4 22.6 %all-gather.4 = bf16[1,1024,128]{2,1,0:T(8,128)(2,1)S(1)} all-gather(bf16[1,32,128]{2,1,0:T(8,128)(2,1)S(1)} %get-tuple-element.10), channel_id=6, replica_groups=mesh['sp'=32,'tp'=4] {'sp'}, dimensions={1}, use_global_device_ids=true | all-gather | bytes 270336 | tf_op jit(solution)/shard_map/all_gather | solution.py:11
  220.0 24.2 %all-gather.7 = bf16[1,128,1024]{1,2,0:T(8,128)(2,1)S(1)} all-gather(bf16[1,128,32]{1,2,0:T(8,128)(2,1)S(1)} %get-tuple-element.7), channel_id=9, replica_groups=mesh['sp'=32,'tp'=4] {'sp'}, dimensions={2}, use_global_device_ids=true | all-gather | bytes 270336 | tf_op jit(solution)/shard_map/all_gather | solution.py:22
  246.1 2.3 collective-permute-start.1
  249.2 0.9 convolution_convert_fusion.1
  250.1 22.8 %reduce-scatter.6.cloned.1.call-done = bf16[128,256]{1,0:T(8,128)(2,1)} async-done(((bf16[128,1024]{1,0:T(8,128)(2,1)}), bf16[128,256]{1,0:T(8,128)(2,1)}) %reduce-scatter.6.cloned.1.call-update) | async-done | bytes 65552 | tf_op jit(solution)/shard_map/reduce_scatter | solution.py:76
  272.9 0.9 fusion.31
  274.5 1.7 reshape.139
  276.2 3.4 all-to-all-start.2
  279.6 24.8 %all-gather.9 = bf16[1,1024,128]{2,1,0:T(8,128)(2,1)S(1)} all-gather(bf16[1,32,128]{2,1,0:T(8,128)(2,1)S(1)} %get-tuple-element.14), channel_id=11, replica_groups=mesh['sp'=32,'tp'=4] {'sp'}, dimensions={1}, use_global_device_ids=true | all-gather | bytes 270336 | tf_op jit(solution)/shard_map/all_gather | solution.py:11
  304.5 24.4 %all-gather.10 = bf16[1,1024,128]{2,1,0:T(8,128)(2,1)S(1)} all-gather(bf16[1,32,128]{2,1,0:T(8,128)(2,1)S(1)} %get-tuple-element.11), channel_id=12, replica_groups=mesh['sp'=32,'tp'=4] {'sp'}, dimensions={1}, use_global_device_ids=true | all-gather | bytes 270336 | tf_op jit(solution)/shard_map/all_gather | solution.py:11
  328.9 22.6 %all-gather.8 = bf16[1,1024,128]{2,1,0:T(8,128)(2,1)S(1)} all-gather(bf16[1,32,128]{2,1,0:T(8,128)(2,1)S(1)} %get-tuple-element.8), channel_id=10, replica_groups=mesh['sp'=32,'tp'=4] {'sp'}, dimensions={1}, use_global_device_ids=true | all-gather | bytes 270336 | tf_op jit(solution)/shard_map/all_gather | solution.py:11
  351.5 24.2 %all-gather.11 = bf16[1,128,1024]{1,2,0:T(8,128)(2,1)S(1)} all-gather(bf16[1,128,32]{1,2,0:T(8,128)(2,1)S(1)} %get-tuple-element.5), channel_id=13, replica_groups=mesh['sp'=32,'tp'=4] {'sp'}, dimensions={2}, use_global_device_ids=true | all-gather | bytes 270336 | tf_op jit(solution)/shard_map/all_gather | solution.py:22
  377.6 2.3 collective-permute-start.2
  380.7 0.9 convolution_convert_fusion
  381.6 22.8 %reduce-scatter.8.cloned.1.call-done = bf16[128,256]{1,0:T(8,128)(2,1)} async-done(((bf16[128,1024]{1,0:T(8,128)(2,1)}), bf16[128,256]{1,0:T(8,128)(2,1)}) %reduce-scatter.8.cloned.1.call-update) | async-done | bytes 65552 | tf_op jit(solution)/shard_map/reduce_scatter | solution.py:76
  404.4 1.5 fusion.30
  (66 shorter events, 10.3 us)
Async XLA Ops:
  9.9 5.6 %copy-start.5 = (f32[3,1024]{1,0:T(4,128)S(1)}, f32[3,1024]{1,0:T(4,128)}, u32[]{:S(2)}) copy-start(f32[3,1024]{1,0:T(4,128)} %param.8) | copy-start | bytes 36868
  9.9 102.7 %all-to-all-start = ((bf16[4,2,16384]{2,1,0:T(2,128)(2,1)}), bf16[4,2,16384]{2,1,0:T(2,128)(2,1)S(1)}, u32[]{:S(2)}, u32[]{:S(2)}) async-start(bf16[4,2,16384]{2,1,0:T(2,128)(2,1)} %reshape.135), calls=%async_computation | async-start | bytes 524288 | tf_op jit(solution)/shard_map/all_to_all | solution.py:40
  15.5 0.7 copy-start.1
  15.5 126.0 %reduce-scatter.4.cloned.1.call-start = ((), (), s32[]{:S(2)}) async-start(), calls=%async_computation.6 | async-start | bytes 327680 | tf_op jit(solution)/shard_map/reduce_scatter | solution.py:76
  16.2 25.3 %copy-start.2 = (bf16[3,32,128]{2,1,0:T(8,128)(2,1)S(1)}, bf16[3,32,128]{2,1,0:T(8,128)(2,1)}, u32[]{:S(2)}) copy-start(bf16[3,32,128]{2,1,0:T(8,128)(2,1)} %param.9) | copy-start | bytes 73732
  41.5 24.2 %copy-start.3 = (bf16[3,32,128]{2,1,0:T(8,128)(2,1)S(1)}, bf16[3,32,128]{2,1,0:T(8,128)(2,1)}, u32[]{:S(2)}) copy-start(bf16[3,32,128]{2,1,0:T(8,128)(2,1)} %param.10) | copy-start | bytes 73732
  65.7 22.6 %copy-start.4 = (bf16[3,128,32]{1,2,0:T(8,128)(2,1)S(1)}, bf16[3,128,32]{1,2,0:T(8,128)(2,1)}, u32[]{:S(2)}) copy-start(bf16[3,128,32]{1,2,0:T(8,128)(2,1)} %param.13) | copy-start | bytes 73732
  88.4 24.2 %copy-start.6 = (f32[3,3,128]{2,1,0:T(4,128)S(1)}, f32[3,3,128]{2,1,0:T(4,128)}, u32[]{:S(2)}) copy-start(f32[3,3,128]{2,1,0:T(4,128)} %param.12) | copy-start | bytes 13828
  114.5 3.1 collective-permute-start
  118.5 22.9 %copy-start = (bf16[4,32,256]{2,1,0:T(8,128)(2,1)S(1)}, bf16[4,32,256]{2,1,0:T(8,128)(2,1)}, u32[]{:S(2)}) copy-start(bf16[4,32,256]{2,1,0:T(8,128)(2,1)} %param.7) | copy-start | bytes 196612
  144.7 99.5 %all-to-all-start.1 = ((bf16[4,2,16384]{2,1,0:T(2,128)(2,1)}), bf16[4,2,16384]{2,1,0:T(2,128)(2,1)S(1)}, u32[]{:S(2)}, u32[]{:S(2)}) async-start(bf16[4,2,16384]{2,1,0:T(2,128)(2,1)} %reshape.137), calls=%async_computation.2 | async-start | bytes 524288 | tf_op jit(solution)/shard_map/all_to_all | solution.py:40
  148.1 124.8 %reduce-scatter.6.cloned.1.call-start = ((), (), s32[]{:S(2)}) async-start(), calls=%async_computation.7 | async-start | bytes 327680 | tf_op jit(solution)/shard_map/reduce_scatter | solution.py:76
  246.1 3.1 collective-permute-start.1
  276.2 99.5 %all-to-all-start.2 = ((bf16[4,2,16384]{2,1,0:T(2,128)(2,1)}), bf16[4,2,16384]{2,1,0:T(2,128)(2,1)S(1)}, u32[]{:S(2)}, u32[]{:S(2)}) async-start(bf16[4,2,16384]{2,1,0:T(2,128)(2,1)} %reshape.139), calls=%async_computation.4 | async-start | bytes 524288 | tf_op jit(solution)/shard_map/all_to_all | solution.py:40
  279.6 124.8 %reduce-scatter.8.cloned.1.call-start = ((), (), s32[]{:S(2)}) async-start(), calls=%async_computation.8 | async-start | bytes 327680 | tf_op jit(solution)/shard_map/reduce_scatter | solution.py:76
  377.6 3.1 collective-permute-start.2
Sparse Core Ops, SparseCore 0:
  118.7 22.7 reduce-scatter.3
  250.2 22.6 reduce-scatter.5
  381.7 22.6 reduce-scatter.7
